TPU v7x, 32 devices: a whole 2x2x4 slice. The times are simulated.
32 devices in a mesh: rep: 2 (over x), fs: 8 (over z, y), tp: 2 (over core).
Axes of the slice: x: 2, y: 2, z: 4, core: 2. Of those that a mesh axis runs over, the one named last changes fastest.
Arguments:
- tokens: bfloat16 [8192, 2048], P(('rep', 'fs'), 'tp'), may hold values from -6 to 6
- mix_gain: float32 [2048], replicated, may hold values from 0.1 to 1.9
- query_w: bfloat16 [2048, 2048], P('fs', 'tp'), may hold values from -0.125 to 0.125
- key_w: bfloat16 [2048, 2048], P('fs', 'tp'), may hold values from -0.125 to 0.125
- value_w: bfloat16 [2048, 4096], P('fs', 'tp'), may hold values from -0.125 to 0.125
- head_gain: float32 [8, 512], replicated, may hold values from 0.1 to 1.9
- out_w: bfloat16 [4096, 2048], P('tp', 'fs'), may hold values from -0.09375 to 0.09375
- chan_gain: float32 [2048], replicated, may hold values from 0.1 to 1.9
- up_w: bfloat16 [2048, 4096], P('fs', 'tp'), may hold values from -0.125 to 0.125
- down_w: bfloat16 [4096, 2048], P('tp', 'fs'), may hold values from -0.09375 to 0.09375
Outputs:
- layer_out: bfloat16 [8192, 2048], P(('rep', 'fs'), 'tp')
All inputs are finite; a program needn't handle non-finite values.
Results may differ from a plain program's by a relative error of at most 0.019.
Values may be sent and summed in bfloat16 or wider, within the bound.
A program may use at most 128 MiB of HBM per device.

v0:
```python
import functools

import jax
import jax.numpy as jnp
import numpy as np
from jax import lax
from jax.experimental import pallas as pl
from jax.experimental.pallas import tpu as pltpu
from jax.sharding import PartitionSpec as P


DK = 256
DV = 512
BLOCK = 128


EPS = 1e-06
HEAD_EPS = 0.05
THETA = 10000.0


def norm_rows(rows, gain):
    values = rows.astype(jnp.float32)
    scale = lax.rsqrt(jnp.mean(values * values, axis=-1, keepdims=True) + EPS)
    return (values * scale * gain).astype(jnp.bfloat16)


def rotate(field, places):
    half = field.shape[-1] // 2
    inverse = THETA ** (-jnp.arange(half, dtype=jnp.float32) / half)
    angles = places[:, None] * inverse
    cosine = jnp.cos(angles)[:, None, :]
    sine = jnp.sin(angles)[:, None, :]
    first = field[..., :half]
    second = field[..., half:]
    return jnp.concatenate(
        [first * cosine - second * sine, second * cosine + first * sine], axis=-1
    )


def retain(query, keys, values, log_rate):
    count = query.shape[0] // BLOCK
    q_blocks = query.reshape(count, BLOCK, query.shape[1])
    k_blocks = keys.reshape(count, BLOCK, keys.shape[1])
    v_blocks = values.reshape(count, BLOCK, values.shape[1])
    place = jnp.arange(BLOCK, dtype=jnp.float32)
    offset = place[:, None] - place[None, :]
    mask = jnp.where(offset >= 0, jnp.exp(log_rate * jnp.maximum(offset, 0.0)), 0.0)
    q_decay = jnp.exp(log_rate * (place + 1.0))
    k_decay = jnp.exp(log_rate * (BLOCK - 1.0 - place))
    block_decay = jnp.exp(log_rate * BLOCK)

    def advance(state, item):
        q_part, k_part, v_part = item
        scores = jnp.dot(q_part, k_part.T, preferred_element_type=jnp.float32)
        weights = (scores * mask).astype(jnp.bfloat16)
        result = jnp.dot(weights, v_part, preferred_element_type=jnp.float32)
        q_scaled = (q_part.astype(jnp.float32) * q_decay[:, None]).astype(jnp.bfloat16)
        result = result + jnp.dot(
            q_scaled, state.astype(jnp.bfloat16), preferred_element_type=jnp.float32
        )
        k_scaled = (k_part.astype(jnp.float32) * k_decay[:, None]).astype(jnp.bfloat16)
        state = state * block_decay + jnp.dot(
            k_scaled.T, v_part, preferred_element_type=jnp.float32
        )
        return (state, result)

    start = jnp.zeros((query.shape[1], values.shape[1]), jnp.float32)
    _, outputs = lax.scan(advance, start, (q_blocks, k_blocks, v_blocks))
    return outputs.reshape(count * BLOCK, values.shape[1])


def shards(tokens, mix_gain, query_w, key_w, value_w, head_gain, out_w, chan_gain, up_w, down_w):
    rows = tokens.shape[0]
    local = query_w.shape[1] // DK
    whole = lax.all_gather(tokens, "tp", axis=1, tiled=True)
    normed = norm_rows(whole, mix_gain)
    pieces = (
        lax.all_gather(query_w, "fs", axis=0, tiled=True),
        lax.all_gather(key_w, "fs", axis=0, tiled=True),
        lax.all_gather(value_w, "fs", axis=0, tiled=True),
    )
    inputs = normed
    qraw, kraw, vraw = tuple(
        (jnp.dot(inputs, piece, preferred_element_type=jnp.float32) for piece in pieces)
    )
    places = jnp.arange(rows, dtype=jnp.int32).astype(jnp.float32)
    query = rotate(qraw.reshape(rows, local, DK), places).astype(jnp.bfloat16)
    keys = (rotate(kraw.reshape(rows, local, DK), places) * DK ** (-0.5)).astype(jnp.bfloat16)
    values = vraw.reshape(rows, local, DV).astype(jnp.bfloat16)
    first_head = lax.axis_index("tp") * local
    heads = (first_head + jnp.arange(local, dtype=jnp.int32)).astype(jnp.float32)
    log_rate = jnp.log1p(-jnp.exp2(-5.0 - heads))
    retained = jax.vmap(retain, in_axes=(1, 1, 1, 0), out_axes=1)(query, keys, values, log_rate)
    gains = lax.dynamic_slice_in_dim(head_gain, first_head, local, 0)
    scale = lax.rsqrt(jnp.mean(retained * retained, axis=-1, keepdims=True) + HEAD_EPS)
    head_out = (retained * scale * gains).astype(jnp.bfloat16).reshape(rows, local * DV)
    mixer_terms = jnp.dot(
        head_out,
        lax.all_gather(out_w, "fs", axis=1, tiled=True),
        preferred_element_type=jnp.float32,
    )
    mixed = lax.psum_scatter(
        mixer_terms.astype(jnp.bfloat16), "tp", scatter_dimension=1, tiled=True
    ).astype(jnp.float32)
    middle = (tokens.astype(jnp.float32) + mixed).astype(jnp.bfloat16)
    whole_middle = lax.all_gather(middle, "tp", axis=1, tiled=True)
    chan_normed = norm_rows(whole_middle, chan_gain)
    inputs = chan_normed
    upward = jnp.dot(
        inputs, lax.all_gather(up_w, "fs", axis=0, tiled=True), preferred_element_type=jnp.float32
    )
    hidden = jnp.square(jax.nn.relu(upward)).astype(jnp.bfloat16)
    chan_terms = jnp.dot(
        hidden, lax.all_gather(down_w, "fs", axis=1, tiled=True), preferred_element_type=jnp.float32
    )
    channel = lax.psum_scatter(
        chan_terms.astype(jnp.bfloat16), "tp", scatter_dimension=1, tiled=True
    ).astype(jnp.float32)
    return (middle.astype(jnp.float32) + channel).astype(jnp.bfloat16)


MESH = pl.DeviceIdType.MESH
QK, VV, OUT, UP, DOWN = range(5)
KINDS = 5
LAG = 2


def loop(count, body):
    def step(index, carry):
        body(index)
        return carry

    lax.fori_loop(0, count, step, 0)


def aligned(start, size):
    return pl.ds(pl.multiple_of(start, size), size)


def mm(left, right):
    return jnp.dot(left, right, preferred_element_type=jnp.float32)


def fused_kernel(count, *refs):
    (
        tokens, query_w, key_w, value_w, out_w, up_w, down_w,
        mix_gain_in, chan_gain_in, head_gain_in, cosine_in, sine_in, rate_in,
        result,
        w_qk, w_v, w_out, w_up, w_down,
        raw, normed, acc, query, keys, values, scores, hidden,
        core_out, core_in, chip_out, chip_in, middle, last_out, last_in,
        mix_gain, chan_gain, head_gain, cosine, sine, rates,
        line_send, line_recv, cross_send, cross_recv, pair_send, pair_recv, local_sem,
        token_send, token_recv, token_local, table_sem,
        core_send, core_recv, chip_send, chip_recv, mid_send, mid_recv,
        end_core_send, end_core_recv, end_send, end_recv, result_sem,
    ) = refs
    bf16, f32 = jnp.bfloat16, jnp.float32
    rows, width = tokens.shape
    planes = count // 2
    total = 2 * rows
    full = 2 * width
    share = full // count
    per_half = count // 2
    dk, dv = DK, DV
    local = query_w.shape[1] // dk // 2
    place = lax.axis_index("fs")
    z, y = place // 2, place % 2
    x = lax.axis_index("rep")
    c = lax.axis_index("tp")
    partner = {"fs": 2 * z + 1 - y}
    twin = {"rep": 1 - x}
    sibling = {"tp": 1 - c}
    first_head = (2 * c + y) * local

    weights = (w_qk, w_v, w_out, w_up, w_down)
    by_rows = (True, True, False, True, False)
    half_q = query_w.shape[1] // 2
    subs = (
        ((query_w, 0, half_q), (key_w, half_q, half_q)),
        ((value_w, 0, value_w.shape[1] // 2),),
        ((out_w, 0, 0),),
        ((up_w, 0, up_w.shape[1] // 2),),
        ((down_w, 0, 0),),
    )

    def region(kind, origin, part):
        ref = weights[kind]
        if by_rows[kind]:
            size = ref.shape[0] // count // 2
            return ref.at[aligned(origin * (2 * size) + part * size, size), :]
        size = ref.shape[1] // 2
        return ref.at[origin, aligned(part * size, size), :]

    def piece_origin(plane, order):
        return 2 * plane + (y if order == 0 else 1 - y)

    def own_copy(kind, sub):
        source, offset, size = subs[kind][sub]
        ref = weights[kind]
        if by_rows[kind]:
            span = source.shape[0]
            return pltpu.make_async_copy(
                source.at[:, aligned(y * size, size)],
                ref.at[aligned(place * span, span), pl.ds(offset, size)],
                local_sem.at[kind, sub],
            )
        span = source.shape[0] // 2
        return pltpu.make_async_copy(
            source.at[aligned(y * span, span), :], ref.at[place], local_sem.at[kind, sub]
        )

    def pair_copy(kind, part, sub):
        source, offset, size = subs[kind][sub]
        ref = weights[kind]
        if by_rows[kind]:
            span = source.shape[0] // 2
            src = source.at[aligned(part * span, span), aligned((1 - y) * size, size)]
            dst = ref.at[aligned(place * (2 * span) + part * span, span), pl.ds(offset, size)]
        else:
            span = source.shape[0] // 4
            src = source.at[aligned((1 - y) * (2 * span) + part * span, span), :]
            dst = ref.at[place, aligned(part * span, span), :]
        return pltpu.make_async_remote_copy(
            src_ref=src, dst_ref=dst,
            send_sem=pair_send.at[kind, part, sub], recv_sem=pair_recv.at[kind, part, sub],
            device_id=partner, device_id_type=MESH,
        )

    def pair_wait(kind, part):
        for sub in range(len(subs[kind])):
            pair_copy(kind, part, sub).wait_recv()

    def line_copy(kind, plane, order, slot, target):
        spot = region(kind, piece_origin(plane, order), x)
        return pltpu.make_async_remote_copy(
            src_ref=spot, dst_ref=spot,
            send_sem=line_send.at[kind, plane, order, slot],
            recv_sem=line_recv.at[kind, plane, order],
            device_id={"fs": target}, device_id_type=MESH,
        )

    def cross_copy(kind, plane, order, part):
        spot = region(kind, piece_origin(plane, order), part)
        return pltpu.make_async_remote_copy(
            src_ref=spot, dst_ref=spot,
            send_sem=cross_send.at[kind, plane, order],
            recv_sem=cross_recv.at[kind, plane, order],
            device_id=twin, device_id_type=MESH,
        )

    orders = [
        sorted(range(planes), key=lambda p: (abs(p - here), (p < here) == (2 * here < planes)))[1:]
        for here in range(planes)
    ]

    def plane_at(step):
        found = jnp.int32(0)
        for here in range(planes):
            found = jnp.where(z == here, jnp.int32(orders[here][step]), found)
        return found

    far = [plane_at(step) for step in range(planes - 1)]

    def forward_way(plane):
        way = jnp.where(plane < z, 1, -1)
        ahead = z + way
        return (ahead >= 0) & (ahead < planes), place + 2 * way

    def send_own(kind, order):
        @pl.when(z < planes - 1)
        def _():
            line_copy(kind, z, order, 0, place + 2).start()

        @pl.when(z > 0)
        def _():
            line_copy(kind, z, order, 1, place - 2).start()

    def begin_local(kind):
        for sub in range(len(subs[kind])):
            own_copy(kind, sub).start()

    def begin_line(kind):
        for sub in range(len(subs[kind])):
            own_copy(kind, sub).wait()
        send_own(kind, 0)

    def begin_pair(kind, part):
        for sub in range(len(subs[kind])):
            pair_copy(kind, part, sub).start()

    def pair_line(kind):
        pair_wait(kind, x)
        send_own(kind, 1)

    def service(kind, step, order):
        plane = far[step]
        line_copy(kind, plane, order, 0, place).wait_recv()
        going, target = forward_way(plane)

        @pl.when(going)
        def _():
            line_copy(kind, plane, order, 0, target).start()

        cross_copy(kind, plane, order, x).start()

    def arrived(kind, step, order):
        cross_copy(kind, far[step], order, 1 - x).wait_recv()

    def token_copy(index):
        own = raw.at[y, c]
        if index == 0:
            spot, target = own, sibling
        elif index == 1:
            spot, target = own, partner
        else:
            spot, target = raw.at[1 - y, c], sibling
        return pltpu.make_async_remote_copy(
            src_ref=spot, dst_ref=spot, send_sem=token_send.at[index],
            recv_sem=token_recv.at[index], device_id=target, device_id_type=MESH,
        )

    tables = (
        (mix_gain_in, mix_gain), (chan_gain_in, chan_gain), (head_gain_in, head_gain),
        (cosine_in, cosine), (sine_in, sine), (rate_in, rates),
    )

    def table_copy(index):
        return pltpu.make_async_copy(tables[index][0], tables[index][1], table_sem.at[index])

    own_tokens = pltpu.make_async_copy(tokens, raw.at[y, c], token_local)

    def norm_first():
        size = 64

        def tile(index):
            for p in range(2):
                span = aligned(index * size, size)
                left = raw[p, 0, span, :].astype(f32)
                right = raw[p, 1, span, :].astype(f32)
                mean = (
                    jnp.sum(left * left, axis=-1, keepdims=True)
                    + jnp.sum(right * right, axis=-1, keepdims=True)
                ) / full
                scale = lax.rsqrt(mean + EPS)
                put = aligned(p * rows + index * size, size)
                normed[put, :width] = (left * scale * mix_gain[:, :width]).astype(bf16)
                normed[put, width:] = (right * scale * mix_gain[:, width:]).astype(bf16)

        loop(rows // size, tile)

    def accumulate(kind, origin, first):
        ref = weights[kind]
        base = 0 if kind == QK else w_qk.shape[1]
        high, wide = min(256, total), min(512, ref.shape[1])
        across = ref.shape[1] // wide

        def tile(index):
            span = aligned(index // across * high, high)
            right = ref[aligned(origin * share, share), aligned(index % across * wide, wide)]
            term = mm(normed[span, aligned(origin * share, share)], right)
            put = aligned(base + index % across * wide, wide)
            if first:
                acc[span, put] = term
            else:
                acc[span, put] += term

        loop(total // high * across, tile)

    def turn():
        size = 128
        half = dk // 2

        def tile(index):
            for p in range(2):
                inner = aligned(index * size, size)
                span = aligned(p * rows + index * size, size)
                cos, sin = cosine[inner, :], sine[inner, :]
                for head in range(local):
                    for base, ref, scale in ((0, query, None), (half_q, keys, dk ** (-0.5))):
                        at = head * dk
                        one = acc[span, base + at : base + at + half]
                        two = acc[span, base + at + half : base + at + dk]
                        low, top = one * cos - two * sin, two * cos + one * sin
                        if scale is not None:
                            low, top = low * scale, top * scale
                        ref[span, at : at + half] = low.astype(bf16)
                        ref[span, at + half : at + dk] = top.astype(bf16)

        loop(rows // size, tile)

    strip = min(256, rows)

    def score(p, head):
        rate = rates[pl.ds(first_head + head, 1), 0:1]
        lanes = slice(head * dk, (head + 1) * dk)
        for block in range(rows // strip):
            seen = (block + 1) * strip
            q_part = query[p * rows + block * strip : p * rows + seen, lanes]
            k_part = keys[p * rows : p * rows + seen, lanes]
            product = lax.dot_general(
                q_part, k_part, (((1,), (1,)), ((), ())), preferred_element_type=f32
            )
            offset = (
                lax.broadcasted_iota(jnp.int32, (strip, seen), 0)
                - lax.broadcasted_iota(jnp.int32, (strip, seen), 1)
                + block * strip
            )
            decay = jnp.exp(rate * jnp.maximum(offset, 0).astype(f32))
            decay = jnp.where(offset >= 0, decay, 0.0)
            scores[p * local + head, block * strip : seen, :seen] = (product * decay).astype(bf16)

    def take_values():
        size = 128

        def tile(index):
            span = aligned(index * size, size)
            values[span, :] = acc[span, w_qk.shape[1] :].astype(bf16)

        loop(total // size, tile)

    def retain_head(p, head):
        gain = head_gain[pl.ds(first_head + head, 1), :]
        lanes = slice(head * dv, (head + 1) * dv)
        for block in range(rows // strip):
            seen = (block + 1) * strip
            got = mm(
                scores[p * local + head, block * strip : seen, :seen],
                values[p * rows : p * rows + seen, lanes],
            )
            mean = jnp.sum(got * got, axis=-1, keepdims=True) / dv
            scale = lax.rsqrt(mean + HEAD_EPS)
            hidden[p * rows + block * strip : p * rows + seen, lanes] = (
                got * scale * gain
            ).astype(bf16)

    high = min(256, total)

    def mine(origin):
        return origin // per_half == c

    def lane(origin):
        return aligned(origin % per_half * share, share)

    def core_copy(plane):
        first = 2 * plane % per_half
        return pltpu.make_async_remote_copy(
            src_ref=core_out.at[pl.ds(first, 2)], dst_ref=core_in.at[pl.ds(first, 2)],
            send_sem=core_send.at[first // 2], recv_sem=core_recv.at[first // 2],
            device_id=sibling, device_id_type=MESH,
        )

    def chip_copy(plane):
        first = 2 * plane % per_half
        return pltpu.make_async_remote_copy(
            src_ref=chip_out.at[pl.ds(first, 2)], dst_ref=chip_in.at[pl.ds(first, 2)],
            send_sem=chip_send.at[first // 2], recv_sem=chip_recv.at[first // 2],
            device_id=partner, device_id_type=MESH,
        )

    def middle_copy(plane):
        spot = middle.at[pl.ds(2 * plane, 2)]
        return pltpu.make_async_remote_copy(
            src_ref=spot, dst_ref=spot, send_sem=mid_send.at[plane], recv_sem=mid_recv.at[plane],
            device_id=sibling, device_id_type=MESH,
        )

    def product(ref, origin, keep):
        def tile(index):
            span = aligned(index * high, high)
            term = mm(hidden[span, :], ref[origin])
            if keep:
                acc[span, lane(origin)] = term
            else:
                core_out[origin % per_half, span, :] = term.astype(bf16)

        loop(total // high, tile)

    def mix_partial(plane):
        @pl.when(mine(2 * plane))
        def _():
            for pick in range(2):
                product(w_out, 2 * plane + pick, True)

        @pl.when(jnp.logical_not(mine(2 * plane)))
        def _():
            for pick in range(2):
                product(w_out, 2 * plane + pick, False)
            core_copy(plane).start()

    def mix_combine(plane):
        @pl.when(mine(2 * plane))
        def _():
            core_copy(plane).wait_recv()
            for pick in range(2):
                origin = 2 * plane + pick

                def tile(index, origin=origin):
                    span = aligned(index * high, high)
                    chip_out[origin % per_half, span, :] = (
                        acc[span, lane(origin)] + core_in[origin % per_half, span, :].astype(f32)
                    ).astype(bf16)

                loop(total // high, tile)
            chip_copy(plane).start()

    def mix_finish(plane):
        @pl.when(mine(2 * plane))
        def _():
            chip_copy(plane).wait_recv()
            for pick in range(2):
                origin = 2 * plane + pick
                for p in range(2):

                    def tile(index, origin=origin, p=p):
                        inner = aligned(index * high, high)
                        span = aligned(p * rows + index * high, high)
                        at = origin % per_half
                        mixed = chip_out[at, span, :].astype(f32) + chip_in[at, span, :].astype(f32)
                        middle[origin, span, :] = (
                            raw[p, c, inner, lane(origin)].astype(f32) + mixed
                        ).astype(bf16)

                    loop(rows // high, tile)
            middle_copy(plane).start()

    def mix_settle(plane):
        @pl.when(jnp.logical_not(mine(2 * plane)))
        def _():
            middle_copy(plane).wait_recv()

    def norm_second():
        size = 64

        def tile(index):
            span = aligned(index * size, size)
            strips = [middle[origin, span, :].astype(f32) for origin in range(count)]
            mean = sum(jnp.sum(s * s, axis=-1, keepdims=True) for s in strips) / full
            scale = lax.rsqrt(mean + EPS)
            for origin in range(count):
                lanes = slice(origin * share, (origin + 1) * share)
                normed[span, lanes] = (strips[origin] * scale * chan_gain[:, lanes]).astype(bf16)

        loop(total // size, tile)

    def upward():
        wide = min(512, w_up.shape[1])
        across = w_up.shape[1] // wide

        def tile(index):
            span = aligned(index // across * high, high)
            lanes = aligned(index % across * wide, wide)
            got = jnp.maximum(mm(normed[span, :], w_up[:, lanes]), 0.0)
            hidden[span, lanes] = (got * got).astype(bf16)

        loop(total // high * across, tile)

    def end_core_copy(origin):
        at = origin % per_half
        return pltpu.make_async_remote_copy(
            src_ref=core_out.at[at], dst_ref=core_in.at[at],
            send_sem=end_core_send.at[at], recv_sem=end_core_recv.at[at],
            device_id=sibling, device_id_type=MESH,
        )

    def end_copy(origin):
        at = origin % per_half
        return pltpu.make_async_remote_copy(
            src_ref=last_out.at[at], dst_ref=last_in.at[at],
            send_sem=end_send.at[at], recv_sem=end_recv.at[at],
            device_id=partner, device_id_type=MESH,
        )

    def result_copy(origin):
        at = origin % per_half
        return pltpu.make_async_copy(
            values.at[aligned(at // 2 * rows, rows), aligned(at % 2 * share, share)],
            result.at[:, lane(origin)],
            result_sem.at[at],
        )

    def end_partial(origin):
        @pl.when(mine(origin))
        def _():
            product(w_down, origin, True)

        @pl.when(jnp.logical_not(mine(origin)))
        def _():
            product(w_down, origin, False)
            end_core_copy(origin).start()

    def end_combine(origin):
        @pl.when(mine(origin))
        def _():
            end_core_copy(origin).wait_recv()
            at = origin % per_half

            def tile(index):
                span = aligned((1 - y) * rows + index * high, high)
                last_out[at, aligned(index * high, high), :] = (
                    acc[span, lane(origin)] + core_in[at, span, :].astype(f32)
                ).astype(bf16)

            loop(rows // high, tile)
            end_copy(origin).start()

    def end_finish(origin):
        @pl.when(mine(origin))
        def _():
            end_copy(origin).wait_recv()
            at = origin % per_half

            def tile(index):
                inner = aligned(index * high, high)
                span = aligned(y * rows + index * high, high)
                added = acc[span, lane(origin)] + core_in[at, span, :].astype(f32)
                added = added + last_in[at, inner, :].astype(f32)
                put = aligned(at // 2 * rows + index * high, high)
                values[put, aligned(at % 2 * share, share)] = (
                    middle[origin, span, :].astype(f32) + added
                ).astype(bf16)

            loop(rows // high, tile)
            result_copy(origin).start()

    begin_local(QK)
    own_tokens.start()
    for index in range(len(tables)):
        table_copy(index).start()
    barrier = pltpu.get_barrier_semaphore()
    for other in (partner, twin, sibling):
        pl.semaphore_signal(barrier, inc=1, device_id=other, device_id_type=MESH)

    @pl.when(z < planes - 1)
    def _():
        pl.semaphore_signal(barrier, inc=1, device_id={"fs": place + 2}, device_id_type=MESH)

    @pl.when(z > 0)
    def _():
        pl.semaphore_signal(barrier, inc=1, device_id={"fs": place - 2}, device_id_type=MESH)

    pl.semaphore_wait(
        barrier, 3 + jnp.where(z < planes - 1, 1, 0) + jnp.where(z > 0, 1, 0)
    )
    begin_pair(QK, x)
    begin_line(QK)
    own_tokens.wait()
    token_copy(0).start()
    token_copy(1).start()
    begin_pair(QK, 1 - x)
    begin_local(VV)
    begin_pair(VV, x)
    begin_pair(VV, 1 - x)
    pair_line(QK)

    def own_pair(kind, task):
        def first():
            task(piece_origin(z, 0))

        def second():
            pair_wait(kind, 1 - x)
            task(piece_origin(z, 1))

        return first, second

    def chunk(kind, step, order, task):
        def run():
            arrived(kind, step, order)
            task(piece_origin(far[step], order))

        return run

    slots = planes - 1
    span = 2 * slots
    plan = {}

    def at(slot, *tasks):
        plan.setdefault(slot, []).extend(tasks)

    def start_tokens():
        token_copy(1).wait_recv()
        token_copy(2).start()

    def first_norm():
        for index in range(len(tables)):
            table_copy(index).wait()
        token_copy(0).wait_recv()
        token_copy(2).wait_recv()
        norm_first()

    last = KINDS * span - 1
    at(4, start_tokens)
    at(5, first_norm)
    own_qk = own_pair(QK, lambda o: accumulate(QK, o, False))
    at(6, lambda: accumulate(QK, piece_origin(z, 0), True), own_qk[1])
    own_v = own_pair(VV, lambda o: accumulate(VV, o, False))
    at(10, lambda: accumulate(VV, piece_origin(z, 0), True), own_v[1])
    for number in range(span):
        step, order = number // 2, number % 2
        at(
            max(number + LAG, 7 + number // 2),
            chunk(QK, step, order, lambda o: accumulate(QK, o, False)),
        )
        at(
            max(number + span + LAG, 10 + number // 2),
            chunk(VV, step, order, lambda o: accumulate(VV, o, False)),
        )
    at(10, turn)
    for p in range(2):
        for head in range(local):
            at(11 + p, functools.partial(score, p, head))
    at(2 * span + LAG - 1, take_values)
    for p in range(2):
        for head in range(local):
            at(2 * span + LAG - 1 + p, functools.partial(retain_head, p, head))
    base = 2 * span + LAG

    def ready(kind, step):
        def run():
            if step < 0:
                pair_wait(kind, 1 - x)
            else:
                for order in range(2):
                    arrived(kind, step, order)

        return run

    def plane_of(step):
        return z if step < 0 else far[step]

    at(base, ready(OUT, -1), lambda: mix_partial(z))
    at(base + 1, lambda: mix_combine(z))
    for step in range(slots):
        when = max(2 * span + 2 * step + 1 + LAG, base + 1)
        at(when, ready(OUT, step), functools.partial(mix_partial, far[step]))
        at(when + 1, functools.partial(mix_combine, far[step]))
    for number in range(planes):
        plane = plane_of(number - 1)
        at(base + 4 + 2 * number, functools.partial(mix_finish, plane))
        at(base + 5 + 2 * number, functools.partial(mix_settle, plane))
    finish = base + 5 + 2 * (planes - 1)

    def third_norm():
        for step in range(-1, slots):
            plane = plane_of(step)

            @pl.when(jnp.logical_not(mine(2 * plane)))
            def _(plane=plane):
                core_copy(plane).wait_send()

        norm_second()

    at(finish, third_norm)

    def up_all():
        for step in range(-1, slots):
            ready(UP, step)()
        upward()

    at(finish + 1, up_all)
    chunks = [piece_origin(z, 0), piece_origin(z, 1)]
    for step in range(slots):
        chunks += [piece_origin(far[step], order) for order in range(2)]

    def down_ready(number):
        def run():
            if number == 1:
                pair_wait(DOWN, 1 - x)
            elif number > 1:
                arrived(DOWN, (number - 2) // 2, number % 2)

        return run

    early = min(count - 2, span + 2 - LAG)
    for number in range(count):
        when = finish + 2 + number // 3
        arrive = 4 * span + (number - 2) + LAG
        when = min(max(when, arrive), last + 1) if number < count - 2 else last + 1
        at(when, down_ready(number), functools.partial(end_partial, chunks[number]))
        at(when if number >= count - 3 else when, functools.partial(end_combine, chunks[number]))
    for number in range(count):
        at(last + 2, functools.partial(end_finish, chunks[number]))

    def run_plan(slot):
        for task in plan.pop(slot, ()):
            task()

    for kind in range(KINDS):
        for step in range(slots):
            for order in range(2):
                if step == slots - 1 and order == 1 and kind + 1 < KINDS:
                    begin_line(kind + 1)
                service(kind, step, order)
                if step == slots - 1 and order == 1 and kind + 1 < KINDS:
                    pair_line(kind + 1)
                if step == 0 and order == 0 and kind + 2 < KINDS:
                    begin_local(kind + 2)
                    begin_pair(kind + 2, x)
                    begin_pair(kind + 2, 1 - x)
                run_plan(kind * span + 2 * step + order)
    for slot in sorted(plan):
        run_plan(slot)
    for kind in range(KINDS):
        for sub in range(len(subs[kind])):
            for part in range(2):
                pair_copy(kind, part, sub).wait_send()
        for order in range(2):

            @pl.when(z < planes - 1)
            def _(kind=kind, order=order):
                line_copy(kind, z, order, 0, place + 2).wait_send()

            @pl.when(z > 0)
            def _(kind=kind, order=order):
                line_copy(kind, z, order, 1, place - 2).wait_send()

        for step in range(slots):
            going, target = forward_way(far[step])
            for order in range(2):

                @pl.when(going)
                def _(kind=kind, order=order, step=step, target=target):
                    line_copy(kind, far[step], order, 0, target).wait_send()

                cross_copy(kind, far[step], order, x).wait_send()
    for index in range(3):
        token_copy(index).wait_send()
    for plane in range(planes):

        @pl.when(mine(2 * plane))
        def _(plane=plane):
            chip_copy(plane).wait_send()
            middle_copy(plane).wait_send()

    for origin in range(count):

        @pl.when(mine(origin))
        def _(origin=origin):
            end_copy(origin).wait_send()
            result_copy(origin).wait()

        @pl.when(jnp.logical_not(mine(origin)))
        def _(origin=origin):
            end_core_copy(origin).wait_send()


def fused_layer(
    count, tokens, mix_gain, query_w, key_w, value_w, head_gain, out_w, chan_gain, up_w, down_w
):
    rows, width = tokens.shape
    total, full = 2 * rows, 2 * width
    planes = count // 2
    per_half = count // 2
    share = full // count
    q_cols = query_w.shape[1] // 2
    v_cols = value_w.shape[1] // 2
    ff_cols = up_w.shape[1] // 2
    local = q_cols // DK
    half = DK // 2
    spots = np.arange(rows, dtype=np.float32)
    inverse = np.float32(THETA) ** (-np.arange(half, dtype=np.float32) / np.float32(half))
    angles = spots[:, None] * inverse.astype(np.float32)
    heads = np.arange(head_gain.shape[0], dtype=np.float32)
    rate = np.log1p(-np.exp2(np.float32(-5.0) - heads)).astype(np.float32)
    rate = np.repeat(rate[:, None], 128, axis=1)
    bf16, f32 = jnp.bfloat16, jnp.float32
    dma = pltpu.SemaphoreType.DMA
    vmem = pltpu.VMEM
    scratch = [
        vmem((full, 2 * q_cols), bf16), vmem((full, v_cols), bf16),
        vmem((count, v_cols, share), bf16), vmem((full, ff_cols), bf16),
        vmem((count, ff_cols, share), bf16),
        vmem((2, 2, rows, width), bf16), vmem((total, full), bf16),
        vmem((total, 2 * q_cols + v_cols), f32),
        vmem((total, q_cols), bf16), vmem((total, q_cols), bf16), vmem((total, v_cols), bf16),
        vmem((2 * local, rows, rows), bf16), vmem((total, v_cols), bf16),
        vmem((per_half, total, share), bf16), vmem((per_half, total, share), bf16),
        vmem((per_half, total, share), bf16), vmem((per_half, total, share), bf16),
        vmem((count, total, share), bf16),
        vmem((per_half, rows, share), bf16), vmem((per_half, rows, share), bf16),
        vmem((1, full), f32), vmem((1, full), f32), vmem(head_gain.shape, f32),
        vmem((rows, half), f32), vmem((rows, half), f32), vmem(rate.shape, f32),
        dma((KINDS, planes, 2, 2)), dma((KINDS, planes, 2)),
        dma((KINDS, planes, 2)), dma((KINDS, planes, 2)),
        dma((KINDS, 2, 2)), dma((KINDS, 2, 2)), dma((KINDS, 2)),
        dma((3,)), dma((3,)), dma, dma((6,)),
        dma((planes // 2,)), dma((planes // 2,)), dma((planes // 2,)), dma((planes // 2,)),
        dma((planes,)), dma((planes,)),
        dma((per_half,)), dma((per_half,)), dma((per_half,)), dma((per_half,)), dma((per_half,)),
    ]
    return pl.pallas_call(
        functools.partial(fused_kernel, count),
        out_shape=jax.ShapeDtypeStruct((rows, width), bf16),
        in_specs=[pl.BlockSpec(memory_space=pl.ANY)] * 13,
        out_specs=pl.BlockSpec(memory_space=pl.ANY),
        scratch_shapes=scratch,
        compiler_params=pltpu.CompilerParams(
            collective_id=0, has_side_effects=True, vmem_limit_bytes=67_043_328
        ),
        name="fused_layer",
    )(
        tokens, query_w, key_w, value_w, out_w, up_w, down_w,
        mix_gain.reshape(1, full), chan_gain.reshape(1, full), head_gain,
        jnp.asarray(np.cos(angles)), jnp.asarray(np.sin(angles)), jnp.asarray(rate),
    )


def solution(mesh):
    placed = (
        P(("rep", "fs"), "tp"),
        P(),
        P("fs", "tp"),
        P("fs", "tp"),
        P("fs", "tp"),
        P(),
        P("tp", "fs"),
        P(),
        P("fs", "tp"),
        P("tp", "fs"),
    )
    parts, tps, count = mesh.shape["rep"], mesh.shape["tp"], mesh.shape["fs"]

    def body(*blocks):
        heads = blocks[2].shape[1] // DK
        if parts == 2 and tps == 2 and count % 4 == 0 and heads % 2 == 0:
            return fused_layer(count, *blocks)
        return shards(*blocks)

    return jax.shard_map(
        body, mesh=mesh, in_specs=placed, out_specs=P(("rep", "fs"), "tp"), check_vma=False
    )
```

profile of v0, /device:TPU:1, one launch (start us, length us, event | category | flops | bytes accessed | tf_op | source)
XLA Modules:
  0.0 202.0 jit_solution(732069853288984488)
XLA Ops:
  0.0 199.7 %fused_layer.1 = bf16[512,1024]{1,0:T(8,128)(2,1)} custom-call(bf16[512,1024]{1,0:T(8,128)(2,1)} %refs_0_.1, bf16[256,1024]{1,0:T(8,128)(2,1)} %refs_1_.1, bf16[256,1024]{1,0:T(8,128)(2,1)} %refs_2_.1, bf16[256,2048]{1,0:T(8,128)(2,1)} %refs_3_.1, bf16[2048,256]{1,0:T(8,128)(2,1)} %refs_4_.1, bf16[256,2048]{1,0:T(8,128)(2,1)} %refs_5_.1, ...), custom_call_target="tpu_custom_call" | custom-call | tf_op jit(solution)/shard_map/fused_layer/pallas_call | solution.py:892
  199.8 2.3 %copy.15 = bf16[512,1024]{1,0:T(8,128)(2,1)} copy(bf16[512,1024]{1,0:T(8,128)(2,1)} %fused_layer.1) | data formatting | bytes 2097152
where the time goes:
time: 202 us
  Pallas kernels  200 us (99%)
  local copies, waits for them, and re-layouts  2.26 us (1%)
    pallas_call x1, Pallas kernels, fused_layer(): pl.pallas_call(functools.partial(fused_kernel, count), out_shape=jax.Shap...  200 us

commit v1 on v0

--- a/solution.py
+++ b/solution.py
@@ -151,7 +151,7 @@
         raw, normed, acc, query, keys, values, scores, hidden,
         core_out, core_in, chip_out, chip_in, middle, last_out, last_in,
         mix_gain, chan_gain, head_gain, cosine, sine, rates,
-        line_send, line_recv, cross_send, cross_recv, pair_send, pair_recv, local_sem,
+        line_send, line_recv, whole_send, whole_recv, cross_send, cross_recv, pair_send, pair_recv, local_sem,
         token_send, token_recv, token_local, table_sem,
         core_send, core_recv, chip_send, chip_recv, mid_send, mid_recv,
         end_core_send, end_core_recv, end_send, end_recv, result_sem,
@@ -250,6 +250,19 @@
             device_id=twin, device_id_type=MESH,
         )
 
+    def whole(kind, plane, order):
+        if (kind, order) != (DOWN, 1):
+            return None
+        return (plane == 0) | (plane == planes - 1)
+
+    def whole_copy(plane, slot, target):
+        spot = region(DOWN, piece_origin(plane, 1), 1 - x)
+        return pltpu.make_async_remote_copy(
+            src_ref=spot, dst_ref=spot,
+            send_sem=whole_send.at[plane, slot], recv_sem=whole_recv.at[plane],
+            device_id={"fs": target}, device_id_type=MESH,
+        )
+
     orders = [
         sorted(range(planes), key=lambda p: (abs(p - here), (p < here) == (2 * here < planes)))[1:]
         for here in range(planes)
@@ -293,6 +306,16 @@
     def pair_line(kind):
         pair_wait(kind, x)
         send_own(kind, 1)
+        if whole(kind, z, 1) is not None:
+            pair_wait(kind, 1 - x)
+
+            @pl.when(z == 0)
+            def _():
+                whole_copy(z, 0, place + 2).start()
+
+            @pl.when(z == planes - 1)
+            def _():
+                whole_copy(z, 1, place - 2).start()
 
     def service(kind, step, order):
         plane = far[step]
@@ -303,10 +326,34 @@
         def _():
             line_copy(kind, plane, order, 0, target).start()
 
-        cross_copy(kind, plane, order, x).start()
+        entire = whole(kind, plane, order)
+        if entire is None:
+            cross_copy(kind, plane, order, x).start()
+            return
+
+        @pl.when(jnp.logical_not(entire))
+        def _():
+            cross_copy(kind, plane, order, x).start()
+
+        @pl.when(entire & going)
+        def _():
+            whole_copy(plane, 0, place).wait_recv()
+            whole_copy(plane, 0, target).start()
 
     def arrived(kind, step, order):
-        cross_copy(kind, far[step], order, 1 - x).wait_recv()
+        plane = far[step]
+        entire = whole(kind, plane, order)
+        if entire is None:
+            cross_copy(kind, plane, order, 1 - x).wait_recv()
+            return
+
+        @pl.when(jnp.logical_not(entire))
+        def _():
+            cross_copy(kind, plane, order, 1 - x).wait_recv()
+
+        @pl.when(entire & jnp.logical_not(forward_way(plane)[0]))
+        def _():
+            whole_copy(plane, 0, place).wait_recv()
 
     def token_copy(index):
         own = raw.at[y, c]
@@ -466,16 +513,16 @@
             device_id=sibling, device_id_type=MESH,
         )
 
-    def product(ref, origin, keep):
+    def product(ref, origin, keep, start=0, size=None):
         def tile(index):
-            span = aligned(index * high, high)
+            span = aligned(start + index * high, high)
             term = mm(hidden[span, :], ref[origin])
             if keep:
                 acc[span, lane(origin)] = term
             else:
                 core_out[origin % per_half, span, :] = term.astype(bf16)
 
-        loop(total // high, tile)
+        loop((total if size is None else size) // high, tile)
 
     def mix_partial(plane):
         @pl.when(mine(2 * plane))
@@ -556,11 +603,12 @@
 
         loop(total // high * across, tile)
 
-    def end_core_copy(origin):
+    def end_core_copy(origin, pick):
         at = origin % per_half
+        span = aligned((1 - y if pick == 0 else y) * rows, rows)
         return pltpu.make_async_remote_copy(
-            src_ref=core_out.at[at], dst_ref=core_in.at[at],
-            send_sem=end_core_send.at[at], recv_sem=end_core_recv.at[at],
+            src_ref=core_out.at[at, span], dst_ref=core_in.at[at, span],
+            send_sem=end_core_send.at[at, pick], recv_sem=end_core_recv.at[at, pick],
             device_id=sibling, device_id_type=MESH,
         )
 
@@ -583,17 +631,18 @@
     def end_partial(origin):
         @pl.when(mine(origin))
         def _():
-            product(w_down, origin, True)
+            product(w_down, origin, True, (1 - y) * rows, rows)
 
         @pl.when(jnp.logical_not(mine(origin)))
         def _():
-            product(w_down, origin, False)
-            end_core_copy(origin).start()
+            for pick in range(2):
+                product(w_down, origin, False, (1 - y if pick == 0 else y) * rows, rows)
+                end_core_copy(origin, pick).start()
 
     def end_combine(origin):
         @pl.when(mine(origin))
         def _():
-            end_core_copy(origin).wait_recv()
+            end_core_copy(origin, 0).wait_recv()
             at = origin % per_half
 
             def tile(index):
@@ -604,10 +653,12 @@
 
             loop(rows // high, tile)
             end_copy(origin).start()
+            product(w_down, origin, True, y * rows, rows)
 
     def end_finish(origin):
         @pl.when(mine(origin))
         def _():
+            end_core_copy(origin, 1).wait_recv()
             end_copy(origin).wait_recv()
             at = origin % per_half
 
@@ -765,22 +816,21 @@
 
     def down_ready(number):
         def run():
-            if number == 1:
-                pair_wait(DOWN, 1 - x)
-            elif number > 1:
+            if number > 1:
                 arrived(DOWN, (number - 2) // 2, number % 2)
 
         return run
 
-    early = min(count - 2, span + 2 - LAG)
     for number in range(count):
         when = finish + 2 + number // 3
         arrive = 4 * span + (number - 2) + LAG
-        when = min(max(when, arrive), last + 1) if number < count - 2 else last + 1
+        when = min(max(when, arrive), last + 1)
+        when = when if number < count - 1 else last + 2
         at(when, down_ready(number), functools.partial(end_partial, chunks[number]))
-        at(when if number >= count - 3 else when, functools.partial(end_combine, chunks[number]))
+        at(when, functools.partial(end_combine, chunks[number]))
     for number in range(count):
-        at(last + 2, functools.partial(end_finish, chunks[number]))
+        early = number < count // 2
+        at(last + 1 if early else last + 3, functools.partial(end_finish, chunks[number]))
 
     def run_plan(slot):
         for task in plan.pop(slot, ()):
@@ -823,7 +873,27 @@
                 def _(kind=kind, order=order, step=step, target=target):
                     line_copy(kind, far[step], order, 0, target).wait_send()
 
-                cross_copy(kind, far[step], order, x).wait_send()
+                entire = whole(kind, far[step], order)
+                if entire is None:
+                    cross_copy(kind, far[step], order, x).wait_send()
+                else:
+
+                    @pl.when(jnp.logical_not(entire))
+                    def _(kind=kind, order=order, step=step):
+                        cross_copy(kind, far[step], order, x).wait_send()
+
+                    @pl.when(entire & going)
+                    def _(step=step, target=target):
+                        whole_copy(far[step], 0, target).wait_send()
+
+    @pl.when(z == 0)
+    def _():
+        whole_copy(z, 0, place + 2).wait_send()
+
+    @pl.when(z == planes - 1)
+    def _():
+        whole_copy(z, 1, place - 2).wait_send()
+
     for index in range(3):
         token_copy(index).wait_send()
     for plane in range(planes):
@@ -842,7 +912,8 @@
 
         @pl.when(jnp.logical_not(mine(origin)))
         def _(origin=origin):
-            end_core_copy(origin).wait_send()
+            for pick in range(2):
+                end_core_copy(origin, pick).wait_send()
 
 
 def fused_layer(
@@ -881,13 +952,14 @@
         vmem((per_half, rows, share), bf16), vmem((per_half, rows, share), bf16),
         vmem((1, full), f32), vmem((1, full), f32), vmem(head_gain.shape, f32),
         vmem((rows, half), f32), vmem((rows, half), f32), vmem(rate.shape, f32),
-        dma((KINDS, planes, 2, 2)), dma((KINDS, planes, 2)),
+        dma((KINDS, planes, 2, 2)), dma((KINDS, planes, 2)), dma((planes, 2)), dma((planes,)),
         dma((KINDS, planes, 2)), dma((KINDS, planes, 2)),
         dma((KINDS, 2, 2)), dma((KINDS, 2, 2)), dma((KINDS, 2)),
         dma((3,)), dma((3,)), dma, dma((6,)),
         dma((planes // 2,)), dma((planes // 2,)), dma((planes // 2,)), dma((planes // 2,)),
         dma((planes,)), dma((planes,)),
-        dma((per_half,)), dma((per_half,)), dma((per_half,)), dma((per_half,)), dma((per_half,)),
+        dma((per_half, 2)), dma((per_half, 2)), dma((per_half,)), dma((per_half,)),
+        dma((per_half,)),
     ]
     return pl.pallas_call(
         functools.partial(fused_kernel, count),

time: 202 us -> 200 us (0.990)
  Pallas kernels: 200 us -> 197 us
    pallas_call x1, Pallas kernels: 200 us -> 197 us  [fused_layer(): pl.pallas_call(functools.partial(fused_kernel, count), out_shape=jax.Shap...]
where the time goes in v1:
time: 200 us; the launch traced here: 199 us
  Pallas kernels  197 us (98%)
  local copies, waits for them, and re-layouts  2.26 us (1%)
    pallas_call x1, Pallas kernels, fused_layer(): pl.pallas_call(functools.partial(fused_kernel, count), out_shape=jax.Shap...  197 us

profile of v1, /device:TPU:1, one launch (start us, length us, event | category | flops | bytes accessed | tf_op | source)
XLA Modules:
  0.0 199.3 jit_solution(18015576609074001174)
XLA Ops:
  0.0 197.1 %fused_layer.1 = bf16[512,1024]{1,0:T(8,128)(2,1)} custom-call(bf16[512,1024]{1,0:T(8,128)(2,1)} %refs_0_.1, bf16[256,1024]{1,0:T(8,128)(2,1)} %refs_1_.1, bf16[256,1024]{1,0:T(8,128)(2,1)} %refs_2_.1, bf16[256,2048]{1,0:T(8,128)(2,1)} %refs_3_.1, bf16[2048,256]{1,0:T(8,128)(2,1)} %refs_4_.1, bf16[256,2048]{1,0:T(8,128)(2,1)} %refs_5_.1, ...), custom_call_target="tpu_custom_call" | custom-call | tf_op jit(solution)/shard_map/fused_layer/pallas_call | solution.py:964
  197.1 2.3 %copy.15 = bf16[512,1024]{1,0:T(8,128)(2,1)} copy(bf16[512,1024]{1,0:T(8,128)(2,1)} %fused_layer.1) | data formatting | bytes 2097152

commit v2 on v1

--- a/solution.py
+++ b/solution.py
@@ -628,16 +628,17 @@
             result_sem.at[at],
         )
 
-    def end_partial(origin):
+    def end_push(origin, pick):
+        start = (1 - y if pick == 0 else y) * rows
+
         @pl.when(mine(origin))
         def _():
-            product(w_down, origin, True, (1 - y) * rows, rows)
+            product(w_down, origin, True, start, rows)
 
         @pl.when(jnp.logical_not(mine(origin)))
         def _():
-            for pick in range(2):
-                product(w_down, origin, False, (1 - y if pick == 0 else y) * rows, rows)
-                end_core_copy(origin, pick).start()
+            product(w_down, origin, False, start, rows)
+            end_core_copy(origin, pick).start()
 
     def end_combine(origin):
         @pl.when(mine(origin))
@@ -653,7 +654,6 @@
 
             loop(rows // high, tile)
             end_copy(origin).start()
-            product(w_down, origin, True, y * rows, rows)
 
     def end_finish(origin):
         @pl.when(mine(origin))
@@ -781,7 +781,7 @@
         return z if step < 0 else far[step]
 
     at(base, ready(OUT, -1), lambda: mix_partial(z))
-    at(base + 1, lambda: mix_combine(z))
+    at(base, lambda: mix_combine(z))
     for step in range(slots):
         when = max(2 * span + 2 * step + 1 + LAG, base + 1)
         at(when, ready(OUT, step), functools.partial(mix_partial, far[step]))
@@ -789,8 +789,9 @@
     for number in range(planes):
         plane = plane_of(number - 1)
         at(base + 4 + 2 * number, functools.partial(mix_finish, plane))
-        at(base + 5 + 2 * number, functools.partial(mix_settle, plane))
-    finish = base + 5 + 2 * (planes - 1)
+        settle = base + 5 + 2 * number if number < planes - 1 else base + 4 + 2 * number
+        at(settle, functools.partial(mix_settle, plane))
+    finish = base + 4 + 2 * (planes - 1)
 
     def third_norm():
         for step in range(-1, slots):
@@ -825,12 +826,27 @@
         when = finish + 2 + number // 3
         arrive = 4 * span + (number - 2) + LAG
         when = min(max(when, arrive), last + 1)
-        when = when if number < count - 1 else last + 2
-        at(when, down_ready(number), functools.partial(end_partial, chunks[number]))
-        at(when, functools.partial(end_combine, chunks[number]))
-    for number in range(count):
-        early = number < count // 2
-        at(last + 1 if early else last + 3, functools.partial(end_finish, chunks[number]))
+        if number < count - 2:
+            chunk_at = chunks[number]
+            at(when, down_ready(number), functools.partial(end_push, chunk_at, 0))
+            at(when, functools.partial(end_combine, chunk_at))
+            at(when, functools.partial(end_push, chunk_at, 1))
+
+    def close(task, *numbers, tail=()):
+        for number in numbers:
+            at(last + 1, functools.partial(task, chunks[number], *tail))
+
+    near, final = count - 2, count - 1
+    close(end_finish, *range(count // 2))
+    at(last + 1, down_ready(final))
+    close(end_push, final, tail=(0,))
+    at(last + 1, down_ready(near))
+    close(end_push, near, tail=(0,))
+    close(end_combine, final)
+    close(end_combine, near)
+    close(end_push, final, tail=(1,))
+    close(end_push, near, tail=(1,))
+    close(end_finish, *range(count // 2, count))
 
     def run_plan(slot):
         for task in plan.pop(slot, ()):

time: 200 us -> 198 us (0.990)
  no operation moved by 1% of the time
where the time goes in v2:
time: 198 us
  Pallas kernels  196 us (99%)
  local copies, waits for them, and re-layouts  2.26 us (1%)
    pallas_call x1, Pallas kernels, fused_layer(): pl.pallas_call(functools.partial(fused_kernel, count), out_shape=jax.Shap...  196 us

profile of v2, /device:TPU:1, one launch (start us, length us, event | category | flops | bytes accessed | tf_op | source)
XLA Modules:
  0.0 198.3 jit_solution(2208647698932215867)
XLA Ops:
  0.0 196.0 %fused_layer.1 = bf16[512,1024]{1,0:T(8,128)(2,1)} custom-call(bf16[512,1024]{1,0:T(8,128)(2,1)} %refs_0_.1, bf16[256,1024]{1,0:T(8,128)(2,1)} %refs_1_.1, bf16[256,1024]{1,0:T(8,128)(2,1)} %refs_2_.1, bf16[256,2048]{1,0:T(8,128)(2,1)} %refs_3_.1, bf16[2048,256]{1,0:T(8,128)(2,1)} %refs_4_.1, bf16[256,2048]{1,0:T(8,128)(2,1)} %refs_5_.1, ...), custom_call_target="tpu_custom_call" | custom-call | tf_op jit(solution)/shard_map/fused_layer/pallas_call | solution.py:980
  196.0 2.3 %copy.15 = bf16[512,1024]{1,0:T(8,128)(2,1)} copy(bf16[512,1024]{1,0:T(8,128)(2,1)} %fused_layer.1) | data formatting | bytes 2097152
